TPU v7x, 512 devices: a 8x2x16 block of a 8x8x16 slice. The times are simulated.
512 devices in a mesh: grp: 2 (over y), sp: 16 (over z), tp: 16 (over x, core).
Axes of the slice: x: 8, y: 2, z: 16, core: 2. Of those that a mesh axis runs over, the one named last changes fastest.
The devices are a block of a 8x8x16 slice.
Arguments:
- target: bfloat16 [4096, 2048], P(('grp', 'sp', 'tp')), parts along dimension 0, may hold values from -5 to 5
- source: bfloat16 [32768, 2048], P(('grp', 'sp', 'tp')), parts along dimension 0, may hold values from -5 to 5
- source_gain: float32 [2048], replicated, may hold values from 0.1 to 1.9
- pre_first: float32 [2048], replicated, may hold values from 0.1 to 1.9
- query_first: bfloat16 [2048, 2048], P(None, 'tp')
- keyval_first: bfloat16 [2048, 1024], P(None, 'tp')
- out_first: bfloat16 [2048, 2048], P('tp'), may hold values from -0.125 to 0.125
- post_first: float32 [2048], replicated, may hold values from 0.1 to 1.9
- ffn_pre: float32 [2048], replicated, may hold values from 0.1 to 1.9
- w_gate: bfloat16 [2048, 2816], P(None, 'tp'), may hold values from -0.125 to 0.125
- w_value: bfloat16 [2048, 2816], P(None, 'tp'), may hold values from -0.125 to 0.125
- conv_gate: float32 [3, 2816], P(None, 'tp'), may hold values from -3.5 to 3.5
- conv_value: float32 [3, 2816], P(None, 'tp'), may hold values from -3.5 to 3.5
- w_down: bfloat16 [2816, 2048], P('tp'), may hold values from -0.109375 to 0.109375
- ffn_post: float32 [2048], replicated, may hold values from 0.1 to 1.9
- pre_second: float32 [2048], replicated, may hold values from 0.1 to 1.9
- query_second: bfloat16 [2048, 2048], P(None, 'tp')
- keyval_second: bfloat16 [2048, 1024], P(None, 'tp')
- out_second: bfloat16 [2048, 2048], P('tp'), may hold values from -0.125 to 0.125
- post_second: float32 [2048], replicated, may hold values from 0.1 to 1.9
Outputs:
- decoded: float32 [4096, 2048], P(('grp', 'sp', 'tp')), parts along dimension 0
There are 2 independent parts, one for each index of `grp`. A program takes and returns all parts, laid end to end along the dimension named above; an argument that names none is the same for every part. Nothing has to cross between parts.
All inputs are finite; a program needn't handle non-finite values.
Results may differ from a plain program's by a relative error of at most 0.04.
Values may be sent and summed in bfloat16 or wider, within the bound.
A program may use at most 128 MiB of HBM per device.

v0:
```python
import jax
import jax.numpy as jnp
from jax import lax
from jax.sharding import PartitionSpec as P

HEAD = 128
KVH = 4


def in_blocks(array, dim, size):
    before, after = (array.shape[:dim], array.shape[dim + 1 :])
    return jnp.moveaxis(array.reshape(*before, size, -1, *after), dim, 0)


def sent_and_summed(array, axis, dim):
    parts = in_blocks(array, dim, lax.axis_size(axis))
    arrived = lax.all_to_all(parts, axis, split_axis=0, concat_axis=0, tiled=True)
    return arrived.astype(jnp.float32).sum(axis=0)


def swapped(block, axis, distance):
    count = lax.axis_size(axis)
    route = []
    for low in range(count):
        high = low | 1 << distance
        if high != low and high < count:
            route += [(low, high), (high, low)]
    return lax.ppermute(block, axis, route)


def in_one_piece(arrays, axis, dim, along):
    both = jnp.concatenate(arrays, axis=along)
    result, at, done = (lax.all_gather(both, axis, axis=dim, tiled=True), 0, [])
    for a in arrays:
        done.append(lax.slice_in_dim(result, at, at + a.shape[along], axis=along))
        at += a.shape[along]
    return tuple(done)


def shifted(value, axis, steps):
    count = lax.axis_size(axis)
    leading, last = (max(0, -steps), min(count, count - steps))
    return lax.ppermute(value, axis, [(source, source + steps) for source in range(leading, last)])


def normed(values, gain):
    widened = values.astype(jnp.float32)
    return widened * lax.rsqrt(jnp.mean(widened * widened, axis=-1, keepdims=True) + 1e-06) * gain


def project_rows(rows_here, weights):
    shard_rows = lax.all_gather(rows_here, "tp", axis=0, tiled=True)
    products = [
        jnp.dot(shard_rows, weight, preferred_element_type=jnp.float32).astype(jnp.bfloat16)
        for weight in weights
    ]
    return jnp.concatenate(products, axis=1)


def summed_rows(parts, weight):
    return sent_and_summed(
        jnp.dot(parts, weight, preferred_element_type=jnp.float32).astype(jnp.bfloat16), "tp", 0
    )


def key_columns(source_rows, keyval_first, keyval_second):
    both_layers = jnp.concatenate([keyval_first, keyval_second], axis=1)
    columns = jnp.einsum(
        "rd,dc->cr",
        lax.all_gather(source_rows, "tp", axis=0, tiled=True),
        both_layers,
        preferred_element_type=jnp.float32,
    ).astype(jnp.bfloat16)
    column_count = keyval_first.shape[1]
    stacked = columns.reshape(2, column_count, columns.shape[1])
    own_index = lax.axis_index("tp")
    doublings = (2 * HEAD // column_count).bit_length() - 1
    for bit_number in range(doublings):
        lower_half = own_index // 2**bit_number % 2 == 0
        half_rows = stacked.shape[2] // 2
        outgoing = jnp.where(lower_half, stacked[:, :, half_rows:], stacked[:, :, :half_rows])
        retained = jnp.where(lower_half, stacked[:, :, :half_rows], stacked[:, :, half_rows:])
        partner = swapped(outgoing, "tp", bit_number)
        stacked = jnp.where(
            lower_half,
            jnp.concatenate([retained, partner], axis=1),
            jnp.concatenate([partner, retained], axis=1),
        )
    return (stacked[:, :HEAD], stacked[:, HEAD:])


def absorber(query_heads, running, shard_pair):
    scale_factor = HEAD ** (-0.5)
    best_score, weight_sum, weighted = running
    key_block, value_block = shard_pair
    scores = (
        jnp.einsum("thd,ds->ths", query_heads, key_block, preferred_element_type=jnp.float32)
        * scale_factor
    )
    newest = jnp.max(scores, axis=2)
    rescale = jnp.exp(best_score - newest)
    weights = jnp.exp(scores - newest[:, :, None])
    weight_sum = weight_sum * rescale + jnp.sum(weights, axis=2)
    weighted = weighted * rescale[:, :, None] + jnp.einsum(
        "ths,ds->thd", weights.astype(jnp.bfloat16), value_block, preferred_element_type=jnp.float32
    )
    return (newest, weight_sum, weighted)


def empty_running(row_count, head_count):
    return (
        jnp.full((row_count, head_count), -jnp.inf, jnp.float32),
        jnp.zeros((row_count, head_count), jnp.float32),
        jnp.zeros((row_count, head_count, HEAD), jnp.float32),
    )


def attend_shares(queries, keys_t, values_t):
    row_count = queries.shape[0]
    own_heads = queries.shape[1] // HEAD
    group_count = lax.axis_size("tp") // KVH
    doublings = group_count.bit_length() - 1
    own_index = lax.axis_index("tp")
    grouped = queries
    for bit_number in range(doublings):
        lower_half = own_index // 2**bit_number % 2 == 0
        partner = swapped(grouped, "tp", bit_number)
        grouped = jnp.where(
            lower_half,
            jnp.concatenate([grouped, partner], axis=1),
            jnp.concatenate([partner, grouped], axis=1),
        )
    head_count = grouped.shape[1] // HEAD
    query_heads = grouped.reshape(row_count, head_count, HEAD)
    best_score, weight_sum, weighted = absorber(
        query_heads,
        empty_running(row_count, head_count),
        in_one_piece((keys_t, values_t), "sp", 1, 0),
    )
    for bit_number in range(doublings):
        other_best, other_sum, other_weighted = (
            swapped(best_score.astype(jnp.bfloat16), "tp", bit_number).astype(best_score.dtype),
            swapped(weight_sum.astype(jnp.bfloat16), "tp", bit_number).astype(weight_sum.dtype),
            swapped(weighted.astype(jnp.bfloat16), "tp", bit_number).astype(weighted.dtype),
        )
        newest = jnp.maximum(best_score, other_best)
        own_scale = jnp.exp(best_score - newest)
        other_scale = jnp.exp(other_best - newest)
        weight_sum = weight_sum * own_scale + other_sum * other_scale
        weighted = weighted * own_scale[:, :, None] + other_weighted * other_scale[:, :, None]
        best_score = newest
    first_head = own_index % group_count * own_heads
    chosen = lax.dynamic_slice_in_dim(weighted, first_head, own_heads, 1)
    chosen_sums = lax.dynamic_slice_in_dim(weight_sum, first_head, own_heads, 1)
    return (
        (chosen / chosen_sums[:, :, None]).reshape(row_count, own_heads * HEAD).astype(jnp.bfloat16)
    )


def causal_mix(rim_rows, up_rows, conv_taps):
    padded = jnp.concatenate([rim_rows, up_rows], axis=0).astype(jnp.float32)
    length = up_rows.shape[0]
    return (
        conv_taps[0] * padded[:length]
        + conv_taps[1] * padded[1 : length + 1]
        + conv_taps[2] * padded[2:]
    )


def per_device(
    target,
    source,
    source_gain,
    pre_first,
    query_first,
    keyval_first,
    out_first,
    post_first,
    ffn_pre,
    w_gate,
    w_value,
    conv_gate,
    conv_value,
    w_down,
    ffn_post,
    pre_second,
    query_second,
    keyval_second,
    out_second,
    post_second,
):
    source_rows = normed(source, source_gain).astype(jnp.bfloat16)
    keys_t, values_t = key_columns(source_rows, keyval_first, keyval_second)

    def attention_layer(stream, pre_gain, w_query, layer_index, w_out, post_gain):
        queries = project_rows(normed(stream, pre_gain).astype(jnp.bfloat16), (w_query,))
        heads = attend_shares(queries, keys_t[layer_index], values_t[layer_index])
        mixed = summed_rows(heads, w_out)
        return stream.astype(jnp.float32) + normed(mixed, post_gain)

    after_first = attention_layer(target, pre_first, query_first, 0, out_first, post_first)
    up_both = project_rows(normed(after_first, ffn_pre).astype(jnp.bfloat16), (w_gate, w_value))
    hidden_width = w_gate.shape[1]
    up_gate = up_both[:, :hidden_width]
    up_value = up_both[:, hidden_width:]
    rim_gate, rim_value = shifted((up_gate[-2:], up_value[-2:]), "sp", 1)
    gated = (
        jax.nn.gelu(causal_mix(rim_gate, up_gate, conv_gate), approximate=True)
        * causal_mix(rim_value, up_value, conv_value)
    ).astype(jnp.bfloat16)
    ffn_sum = summed_rows(gated, w_down)
    after_ffn = after_first + normed(ffn_sum, ffn_post)
    return attention_layer(after_ffn, pre_second, query_second, 1, out_second, post_second)


def solution(mesh):
    placed = (
        P(("grp", "sp", "tp"), None),
        P(("grp", "sp", "tp"), None),
        P(),
        P(),
        P(None, "tp"),
        P(None, "tp"),
        P("tp", None),
        P(),
        P(),
        P(None, "tp"),
        P(None, "tp"),
        P(None, "tp"),
        P(None, "tp"),
        P("tp", None),
        P(),
        P(),
        P(None, "tp"),
        P(None, "tp"),
        P("tp", None),
        P(),
    )
    return jax.shard_map(
        per_device,
        mesh=mesh,
        in_specs=placed,
        out_specs=P(("grp", "sp", "tp"), None),
        check_vma=False,
    )
```

profile of v0, /device:TPU:65, one launch (start us, length us, event | category | flops | bytes accessed | tf_op | source)
XLA Modules:
  0.0 380.8 jit_solution(5917875736320434852)
XLA Ops:
  6.6 1.2 fusion.19
  7.8 1.8 fusion.21
  9.8 83.2 %all-gather.4.cloned.1.call-done = bf16[1024,2048]{1,0:T(8,128)(2,1)} async-done(((bf16[64,2048]{1,0:T(8,128)(2,1)}), bf16[1024,2048]{1,0:T(8,128)(2,1)}) %all-gather.4.cloned.1.call-update) | async-done | bytes 4194320 | tf_op jit(solution)/shard_map/all_gather | solution.py:70
  93.0 3.9 %convolution_convert_fusion.3 = bf16[128,1024]{1,0:T(8,128)(2,1)S(1)} fusion(bf16[1024,2048]{1,0:T(8,128)(2,1)} %all-gather.4.cloned.1.call-done, bf16[2048,64]{0,1:T(8,128)(2,1)} %param.37, bf16[2048,64]{0,1:T(8,128)(2,1)} %param.25), kind=kOutput, calls=%fused_computation.16 | convolution fusion | flops 538050560 | bytes 4980736 | tf_op jit(solution)/shard_map/rd,dc->cr/dot_general | solution.py:68
  96.9 2.2 collective-permute-start.2
  99.1 1.0 collective-permute-done.2
  100.2 3.0 collective-permute-start.3
  103.3 3.7 collective-permute-done.3
  107.0 0.7 slice_bitcast_fusion.9
  107.7 0.7 pad_maximum_fusion
  108.7 18.7 %all_gather.18 = bf16[128,2048]{1,0:T(8,128)(2,1)S(1)} all-gather(bf16[8,2048]{1,0:T(8,128)(2,1)S(1)} %fusion.52), channel_id=1, replica_groups=mesh['grp'=2,'sp'=16,'tp'=16] {'tp'}, dimensions={0}, use_global_device_ids=true | all-gather | bytes 557056 | tf_op jit(solution)/shard_map/all_gather | solution.py:52
  127.7 2.1 collective-permute-start
  129.8 1.0 collective-permute-done
  130.9 2.0 collective-permute-start.1
  132.8 3.5 collective-permute-done.1
  136.4 41.9 %all-gather.6.cloned.1.call-done = bf16[256,4096]{1,0:T(8,128)(2,1)} async-done(((bf16[256,256]{1,0:T(8,128)(2,1)}), bf16[256,4096]{1,0:T(8,128)(2,1)}) %all-gather.6.cloned.1.call-update) | async-done | bytes 2097168 | tf_op jit(solution)/shard_map/all_gather | solution.py:33
  178.3 2.7 multiply_reduce_fusion.1
  181.1 1.5 fusion
  182.7 13.7 %collective-permute-start.4 = (bf16[128,4]{0,1:T(4,128)(2,1)S(1)}, bf16[128,4]{0,1:T(4,128)(2,1)S(1)}, u32[]{:S(2)}, u32[]{:S(2)}) collective-permute-start(bf16[128,4]{0,1:T(4,128)(2,1)S(1)} %get-tuple-element.43), channel_id=1, source_target_pairs={{0,1},{1,0},{2,3},{3,2},{4,5},{5,4},{6,7},{7,6},{8,9},{9,8},{10,11... | collective-permute-start | bytes 3080 | tf_op jit(solution)/shard_map/ppermute | solution.py:28
  196.4 2.0 collective-permute-start.8
  198.4 3.5 collective-permute-start.6
  201.9 2.0 collective-permute-start.9
  203.9 2.4 collective-permute-done.9
  206.2 0.6 multiply_add_fusion.6
  206.8 2.3 fusion.109
  209.2 4.0 %collective-permute-start.5 = (bf16[128,4,128]{2,0,1:T(8,128)(2,1)}, bf16[128,4,128]{2,0,1:T(8,128)(2,1)}, u32[]{:S(2)}, u32[]{:S(2)}) collective-permute-start(bf16[128,4,128]{2,0,1:T(8,128)(2,1)} %get-tuple-element.47), channel_id=1, source_target_pairs={{0,1},{1,0},{2,3},{3,2},{4,5},{5,4},{6,7},{7,6},{8,9},{9,8},{10,11... | collective-permute-start | bytes 393224 | tf_op jit(solution)/shard_map/ppermute | solution.py:28
  213.2 1.3 collective-permute-done.5
  214.5 1.1 fusion.104
  215.6 2.0 collective-permute-start.7
  217.5 0.7 fusion.84
  218.2 4.0 %collective-permute-done.7 = bf16[128,4,128]{2,0,1:T(8,128)(2,1)S(1)} collective-permute-done((bf16[128,4,128]{2,0,1:T(8,128)(2,1)S(1)}, bf16[128,4,128]{2,0,1:T(8,128)(2,1)S(1)}, u32[]{:S(2)}, u32[]{:S(2)}) %collective-permute-start.7) | collective-permute-done | bytes 131104 | tf_op jit(solution)/shard_map/ppermute | solution.py:28
  222.2 1.2 fusion.8
  223.4 6.5 %all-to-all-start = ((bf16[16,8,2048]{2,1,0:T(8,128)(2,1)}), bf16[16,8,2048]{2,1,0:T(8,128)(2,1)S(1)}, u32[]{:S(2)}, u32[]{:S(2)}) async-start(bf16[16,8,2048]{2,1,0:T(8,128)(2,1)} %fusion.8), calls=%async_computation | async-start | bytes 1048576 | tf_op jit(solution)/shard_map/all_to_all | solution.py:17
  230.0 0.8 fusion.105
  230.8 0.8 fusion.106
  231.6 1.5 pad_maximum_fusion.1
  233.2 13.9 %all-to-all-done = bf16[16,8,2048]{2,1,0:T(8,128)(2,1)S(1)} async-done(((bf16[16,8,2048]{2,1,0:T(8,128)(2,1)}), bf16[16,8,2048]{2,1,0:T(8,128)(2,1)S(1)}, u32[]{:S(2)}, u32[]{:S(2)}) %all-to-all-start) | async-done | bytes 524320 | tf_op jit(solution)/shard_map/all_to_all | solution.py:17
  247.6 16.0 %all_gather.21 = bf16[128,2048]{1,0:T(8,128)(2,1)S(1)} all-gather(bf16[8,2048]{1,0:T(8,128)(2,1)S(1)} %multiply_convert_fusion.1), channel_id=1, replica_groups=mesh['grp'=2,'sp'=16,'tp'=16] {'tp'}, dimensions={0}, use_global_device_ids=true | all-gather | bytes 557056 | tf_op jit(solution)/shard_map/all_gather | solution.py:52
  263.6 0.4 convolution_convert_fusion.5
  264.1 3.2 collective-permute-start.10
  267.8 2.1 collective-permute-start.11
  270.0 1.0 collective-permute-done.11
  271.1 0.6 fusion.9
  271.7 23.3 %all_to_all.15 = bf16[16,8,2048]{2,1,0:T(8,128)(2,1)S(1)} all-to-all(bf16[16,8,2048]{2,1,0:T(8,128)(2,1)S(1)} %fusion.9), channel_id=1, replica_groups=mesh['grp'=2,'sp'=16,'tp'=16] {'tp'}, dimensions={0} | all-to-all | bytes 1048576 | tf_op jit(solution)/shard_map/all_to_all | solution.py:17
  295.6 16.0 %all_gather.22 = bf16[128,2048]{1,0:T(8,128)(2,1)S(1)} all-gather(bf16[8,2048]{1,0:T(8,128)(2,1)S(1)} %multiply_convert_fusion), channel_id=1, replica_groups=mesh['grp'=2,'sp'=16,'tp'=16] {'tp'}, dimensions={0}, use_global_device_ids=true | all-gather | bytes 557056 | tf_op jit(solution)/shard_map/all_gather | solution.py:52
  311.9 2.1 collective-permute-start.12
  314.0 1.0 collective-permute-done.12
  315.1 2.2 collective-permute-start.13
  317.3 3.2 collective-permute-done.13
  320.5 2.7 multiply_reduce_fusion
  323.2 1.5 fusion.2
  324.7 3.0 collective-permute-start.14
  327.7 2.0 collective-permute-start.18
  329.7 2.2 collective-permute-start.16
  331.9 3.2 collective-permute-start.19
  335.1 1.2 collective-permute-done.19
  336.3 1.7 fusion.110
  338.0 3.9 %collective-permute-start.15 = (bf16[128,4,128]{2,0,1:T(8,128)(2,1)S(1)}, bf16[128,4,128]{2,0,1:T(8,128)(2,1)S(1)}, u32[]{:S(2)}, u32[]{:S(2)}) collective-permute-start(bf16[128,4,128]{2,0,1:T(8,128)(2,1)S(1)} %get-tuple-element.51), channel_id=1, source_target_pairs={{0,1},{1,0},{2,3},{3,2},{4,5},{5,4},{6,7},{7,6},{8,9},{9,8},{10,11... | collective-permute-start | bytes 393224 | tf_op jit(solution)/shard_map/ppermute | solution.py:28
  341.9 0.9 collective-permute-done.15
  343.0 3.2 collective-permute-start.17
  346.2 3.4 collective-permute-done.17
  349.6 0.4 fusion.10
  350.0 23.3 %all_to_all.16 = bf16[16,8,2048]{2,1,0:T(8,128)(2,1)S(1)} all-to-all(bf16[16,8,2048]{2,1,0:T(8,128)(2,1)S(1)} %fusion.10), channel_id=1, replica_groups=mesh['grp'=2,'sp'=16,'tp'=16] {'tp'}, dimensions={0} | all-to-all | bytes 1048576 | tf_op jit(solution)/shard_map/all_to_all | solution.py:17
  373.5 0.7 multiply_add_fusion.2
  (92 shorter events, 3.9 us)
Async XLA Ops:
  6.5 264.6 %copy-start = (bf16[176,2048]{1,0:T(8,128)(2,1)S(1)}, bf16[176,2048]{1,0:T(8,128)(2,1)}, u32[]{:S(2)}) copy-start(bf16[176,2048]{1,0:T(8,128)(2,1)} %param.33) | copy-start | bytes 2162692
  6.6 101.9 %copy-start.1 = (bf16[8,2048]{1,0:T(8,128)(2,1)S(1)}, bf16[8,2048]{1,0:T(8,128)(2,1)}, u32[]{:S(2)}) copy-start(bf16[8,2048]{1,0:T(8,128)(2,1)} %param.20) | copy-start | bytes 98308
  6.6 102.0 %copy-start.11 = (f32[2048]{0:T(1024)S(1)}, f32[2048]{0:T(1024)}, u32[]{:S(2)}) copy-start(f32[2048]{0:T(1024)} %param.23) | copy-start | bytes 24580
  6.6 120.8 %copy-start.4 = (bf16[2048,128]{1,0:T(8,128)(2,1)S(1)}, bf16[2048,128]{1,0:T(8,128)(2,1)}, u32[]{:S(2)}) copy-start(bf16[2048,128]{1,0:T(8,128)(2,1)} %param.24) | copy-start | bytes 1572868
  6.6 86.4 %all-gather.4.cloned.1.call-start = ((), (), s32[]{:S(2)}) async-start(), calls=%async_computation.3 | async-start | bytes 4456448 | tf_op jit(solution)/shard_map/all_gather | solution.py:70
  9.7 168.6 %all-gather.6.cloned.1.call-start = ((), (), s32[]{:S(2)}) async-start(), calls=%async_computation.4 | async-start | bytes 2228224 | tf_op jit(solution)/shard_map/all_gather | solution.py:33
  96.9 3.3 collective-permute-start.2
  100.2 6.7 %collective-permute-start.3 = (bf16[2,128,256]{2,1,0:T(8,128)(2,1)S(1)}, bf16[2,128,256]{2,1,0:T(8,128)(2,1)S(1)}, u32[]{:S(2)}, u32[]{:S(2)}) collective-permute-start(bf16[2,128,256]{2,1,0:T(8,128)(2,1)S(1)} %get-tuple-element.30), channel_id=1, source_target_pairs={{0,2},{2,0},{1,3},{3,1},{4,6},{6,4},{5,7},{7,5},{8,10},{10,8},{9,1... | collective-permute-start | bytes 393224 | tf_op jit(solution)/shard_map/ppermute | solution.py:28
  127.7 3.1 collective-permute-start
  130.9 5.5 %collective-permute-start.1 = (bf16[128,256]{0,1:T(8,128)(2,1)S(1)}, bf16[128,256]{0,1:T(8,128)(2,1)S(1)}, u32[]{:S(2)}, u32[]{:S(2)}) collective-permute-start(bf16[128,256]{0,1:T(8,128)(2,1)S(1)} %maximum_select_fusion.7), channel_id=1, source_target_pairs={{0,2},{2,0},{1,3},{3,1},{4,6},{6,4},{5,7},{7,5},{8,10},{10,8},{9,1... | collective-permute-start | bytes 196616 | tf_op jit(solution)/shard_map/ppermute | solution.py:28
  178.3 28.5 %copy-start.9 = (bf16[256,4096]{1,0:T(8,128)(2,1)S(1)}, bf16[256,4096]{1,0:T(8,128)(2,1)}, u32[]{:S(2)}) copy-start(bf16[256,4096]{1,0:T(8,128)(2,1)} %all-gather.6.cloned.1.call-done) | copy-start | bytes 6291460
  181.1 41.1 %copy-start.5 = (bf16[128,2048]{1,0:T(8,128)(2,1)S(1)}, bf16[128,2048]{1,0:T(8,128)(2,1)}, u32[]{:S(2)}) copy-start(bf16[128,2048]{1,0:T(8,128)(2,1)} %param.26) | copy-start | bytes 1572868
  182.6 64.7 %copy-start.10 = (f32[2048]{0:T(1024)S(1)}, f32[2048]{0:T(1024)}, u32[]{:S(2)}) copy-start(f32[2048]{0:T(1024)} %param.27) | copy-start | bytes 24580
  182.6 64.9 %copy-start.12 = (f32[2048]{0:T(1024)S(1)}, f32[2048]{0:T(1024)}, u32[]{:S(2)}) copy-start(f32[2048]{0:T(1024)} %param.28) | copy-start | bytes 24580
  182.6 81.0 %copy-start.2 = (bf16[2048,176]{0,1:T(8,128)(2,1)S(1)}, bf16[2048,176]{0,1:T(8,128)(2,1)}, u32[]{:S(2)}) copy-start(bf16[2048,176]{0,1:T(8,128)(2,1)} %param.29) | copy-start | bytes 2162692
  182.6 84.7 %copy-start.3 = (bf16[2048,176]{0,1:T(8,128)(2,1)S(1)}, bf16[2048,176]{0,1:T(8,128)(2,1)}, u32[]{:S(2)}) copy-start(bf16[2048,176]{0,1:T(8,128)(2,1)} %param.30) | copy-start | bytes 2162692
  182.7 15.7 %collective-permute-start.4 = (bf16[128,4]{0,1:T(4,128)(2,1)S(1)}, bf16[128,4]{0,1:T(4,128)(2,1)S(1)}, u32[]{:S(2)}, u32[]{:S(2)}) collective-permute-start(bf16[128,4]{0,1:T(4,128)(2,1)S(1)} %get-tuple-element.43), channel_id=1, source_target_pairs={{0,1},{1,0},{2,3},{3,2},{4,5},{5,4},{6,7},{7,6},{8,9},{9,8},{10,11... | collective-permute-start | bytes 3080 | tf_op jit(solution)/shard_map/ppermute | solution.py:28
  196.4 5.5 %collective-permute-start.8 = (bf16[128,4]{0,1:T(4,128)(2,1)S(1)}, bf16[128,4]{0,1:T(4,128)(2,1)S(1)}, u32[]{:S(2)}, u32[]{:S(2)}) collective-permute-start(bf16[128,4]{0,1:T(4,128)(2,1)S(1)} %get-tuple-element.44), channel_id=1, source_target_pairs={{0,1},{1,0},{2,3},{3,2},{4,5},{5,4},{6,7},{7,6},{8,9},{9,8},{10,11... | collective-permute-start | bytes 3080 | tf_op jit(solution)/shard_map/ppermute | solution.py:28
  198.4 5.5 %collective-permute-start.6 = (bf16[128,4]{0,1:T(4,128)(2,1)S(1)}, bf16[128,4]{0,1:T(4,128)(2,1)S(1)}, u32[]{:S(2)}, u32[]{:S(2)}) collective-permute-start(bf16[128,4]{0,1:T(4,128)(2,1)S(1)} %fusion.82), channel_id=1, source_target_pairs={{0,2},{2,0},{1,3},{3,1},{4,6},{6,4},{5,7},{7,5},{8,10},{10,8},{9,1... | collective-permute-start | bytes 3080 | tf_op jit(solution)/shard_map/ppermute | solution.py:28
  201.9 4.3 %collective-permute-start.9 = (bf16[128,4]{0,1:T(4,128)(2,1)S(1)}, bf16[128,4]{0,1:T(4,128)(2,1)S(1)}, u32[]{:S(2)}, u32[]{:S(2)}) collective-permute-start(bf16[128,4]{0,1:T(4,128)(2,1)S(1)} %get-tuple-element.19), channel_id=1, source_target_pairs={{0,2},{2,0},{1,3},{3,1},{4,6},{6,4},{5,7},{7,5},{8,10},{10,8},{9,1... | collective-permute-start | bytes 3080 | tf_op jit(solution)/shard_map/ppermute | solution.py:28
  206.8 88.4 %copy-start.13 = (f32[2048]{0:T(1024)S(1)}, f32[2048]{0:T(1024)}, u32[]{:S(2)}) copy-start(f32[2048]{0:T(1024)} %param.34) | copy-start | bytes 24580
  206.8 88.7 %copy-start.15 = (f32[2048]{0:T(1024)S(1)}, f32[2048]{0:T(1024)}, u32[]{:S(2)}) copy-start(f32[2048]{0:T(1024)} %param.35) | copy-start | bytes 24580
  209.2 102.4 %copy-start.6 = (bf16[2048,128]{1,0:T(8,128)(2,1)S(1)}, bf16[2048,128]{1,0:T(8,128)(2,1)}, u32[]{:S(2)}) copy-start(bf16[2048,128]{1,0:T(8,128)(2,1)} %param.36) | copy-start | bytes 1572868
  209.2 5.3 %collective-permute-start.5 = (bf16[128,4,128]{2,0,1:T(8,128)(2,1)}, bf16[128,4,128]{2,0,1:T(8,128)(2,1)}, u32[]{:S(2)}, u32[]{:S(2)}) collective-permute-start(bf16[128,4,128]{2,0,1:T(8,128)(2,1)} %get-tuple-element.47), channel_id=1, source_target_pairs={{0,1},{1,0},{2,3},{3,2},{4,5},{5,4},{6,7},{7,6},{8,9},{9,8},{10,11... | collective-permute-start | bytes 393224 | tf_op jit(solution)/shard_map/ppermute | solution.py:28
  215.6 6.6 %collective-permute-start.7 = (bf16[128,4,128]{2,0,1:T(8,128)(2,1)S(1)}, bf16[128,4,128]{2,0,1:T(8,128)(2,1)S(1)}, u32[]{:S(2)}, u32[]{:S(2)}) collective-permute-start(bf16[128,4,128]{2,0,1:T(8,128)(2,1)S(1)} %get-tuple-element.23), channel_id=1, source_target_pairs={{0,2},{2,0},{1,3},{3,1},{4,6},{6,4},{5,7},{7,5},{8,10},{10,8},{9,1... | collective-permute-start | bytes 393224 | tf_op jit(solution)/shard_map/ppermute | solution.py:28
  223.4 23.7 %all-to-all-start = ((bf16[16,8,2048]{2,1,0:T(8,128)(2,1)}), bf16[16,8,2048]{2,1,0:T(8,128)(2,1)S(1)}, u32[]{:S(2)}, u32[]{:S(2)}) async-start(bf16[16,8,2048]{2,1,0:T(8,128)(2,1)} %fusion.8), calls=%async_computation | async-start | bytes 1048576 | tf_op jit(solution)/shard_map/all_to_all | solution.py:17
  229.9 87.4 %all-gather.8.cloned.1.call-start = ((), (), s32[]{:S(2)}) async-start(), calls=%async_computation.5 | async-start | bytes 2228224 | tf_op jit(solution)/shard_map/all_gather | solution.py:33
  264.1 5.8 %collective-permute-start.10 = (bf16[2,176]{0,1:T(8,128)(2,1)S(1)}, bf16[2,176]{0,1:T(8,128)(2,1)S(1)}, u32[]{:S(2)}, u32[]{:S(2)}) collective-permute-start(bf16[2,176]{0,1:T(8,128)(2,1)S(1)} %slice.122), channel_id=1, source_target_pairs={{0,16},{16,32},{32,48},{48,64},{64,80},{80,96},{96,112},{112,128},... | collective-permute-start | bytes 2120 | tf_op jit(solution)/shard_map/ppermute | solution.py:43
  267.8 3.2 collective-permute-start.11
  311.9 3.1 collective-permute-start.12
  315.1 5.4 %collective-permute-start.13 = (bf16[128,256]{0,1:T(8,128)(2,1)S(1)}, bf16[128,256]{0,1:T(8,128)(2,1)S(1)}, u32[]{:S(2)}, u32[]{:S(2)}) collective-permute-start(bf16[128,256]{0,1:T(8,128)(2,1)S(1)} %maximum_select_fusion.9), channel_id=1, source_target_pairs={{0,2},{2,0},{1,3},{3,1},{4,6},{6,4},{5,7},{7,5},{8,10},{10,8},{9,1... | collective-permute-start | bytes 196616 | tf_op jit(solution)/shard_map/ppermute | solution.py:28
  320.5 15.8 %copy-start.8 = (bf16[256,4096]{1,0:T(8,128)(2,1)S(1)}, bf16[256,4096]{1,0:T(8,128)(2,1)}, u32[]{:S(2)}) copy-start(bf16[256,4096]{1,0:T(8,128)(2,1)} %all-gather.8.cloned.1.call-done) | copy-start | bytes 6291460
  323.2 26.4 %copy-start.7 = (bf16[128,2048]{1,0:T(8,128)(2,1)S(1)}, bf16[128,2048]{1,0:T(8,128)(2,1)}, u32[]{:S(2)}) copy-start(bf16[128,2048]{1,0:T(8,128)(2,1)} %param.38) | copy-start | bytes 1572868
  324.7 48.8 %copy-start.14 = (f32[2048]{0:T(1024)S(1)}, f32[2048]{0:T(1024)}, u32[]{:S(2)}) copy-start(f32[2048]{0:T(1024)} %param.39) | copy-start | bytes 24580
  324.7 4.9 %collective-permute-start.14 = (bf16[128,4]{0,1:T(4,128)(2,1)S(1)}, bf16[128,4]{0,1:T(4,128)(2,1)S(1)}, u32[]{:S(2)}, u32[]{:S(2)}) collective-permute-start(bf16[128,4]{0,1:T(4,128)(2,1)S(1)} %get-tuple-element.40), channel_id=1, source_target_pairs={{0,1},{1,0},{2,3},{3,2},{4,5},{5,4},{6,7},{7,6},{8,9},{9,8},{10,11... | collective-permute-start | bytes 3080 | tf_op jit(solution)/shard_map/ppermute | solution.py:28
  327.7 4.2 %collective-permute-start.18 = (bf16[128,4]{0,1:T(4,128)(2,1)S(1)}, bf16[128,4]{0,1:T(4,128)(2,1)S(1)}, u32[]{:S(2)}, u32[]{:S(2)}) collective-permute-start(bf16[128,4]{0,1:T(4,128)(2,1)S(1)} %get-tuple-element.41), channel_id=1, source_target_pairs={{0,1},{1,0},{2,3},{3,2},{4,5},{5,4},{6,7},{7,6},{8,9},{9,8},{10,11... | collective-permute-start | bytes 3080 | tf_op jit(solution)/shard_map/ppermute | solution.py:28
  329.7 5.4 %collective-permute-start.16 = (bf16[128,4]{0,1:T(4,128)(2,1)S(1)}, bf16[128,4]{0,1:T(4,128)(2,1)S(1)}, u32[]{:S(2)}, u32[]{:S(2)}) collective-permute-start(bf16[128,4]{0,1:T(4,128)(2,1)S(1)} %fusion.83), channel_id=1, source_target_pairs={{0,2},{2,0},{1,3},{3,1},{4,6},{6,4},{5,7},{7,5},{8,10},{10,8},{9,1... | collective-permute-start | bytes 3080 | tf_op jit(solution)/shard_map/ppermute | solution.py:28
  331.9 4.3 %collective-permute-start.19 = (bf16[128,4]{0,1:T(4,128)(2,1)S(1)}, bf16[128,4]{0,1:T(4,128)(2,1)S(1)}, u32[]{:S(2)}, u32[]{:S(2)}) collective-permute-start(bf16[128,4]{0,1:T(4,128)(2,1)S(1)} %get-tuple-element.8), channel_id=1, source_target_pairs={{0,2},{2,0},{1,3},{3,1},{4,6},{6,4},{5,7},{7,5},{8,10},{10,8},{9,1... | collective-permute-start | bytes 3080 | tf_op jit(solution)/shard_map/ppermute | solution.py:28
  338.0 4.8 %collective-permute-start.15 = (bf16[128,4,128]{2,0,1:T(8,128)(2,1)S(1)}, bf16[128,4,128]{2,0,1:T(8,128)(2,1)S(1)}, u32[]{:S(2)}, u32[]{:S(2)}) collective-permute-start(bf16[128,4,128]{2,0,1:T(8,128)(2,1)S(1)} %get-tuple-element.51), channel_id=1, source_target_pairs={{0,1},{1,0},{2,3},{3,2},{4,5},{5,4},{6,7},{7,6},{8,9},{9,8},{10,11... | collective-permute-start | bytes 393224 | tf_op jit(solution)/shard_map/ppermute | solution.py:28
  343.0 6.6 %collective-permute-start.17 = (bf16[128,4,128]{2,0,1:T(8,128)(2,1)S(1)}, bf16[128,4,128]{2,0,1:T(8,128)(2,1)S(1)}, u32[]{:S(2)}, u32[]{:S(2)}) collective-permute-start(bf16[128,4,128]{2,0,1:T(8,128)(2,1)S(1)} %get-tuple-element.12), channel_id=1, source_target_pairs={{0,2},{2,0},{1,3},{3,1},{4,6},{6,4},{5,7},{7,5},{8,10},{10,8},{9,1... | collective-permute-start | bytes 393224 | tf_op jit(solution)/shard_map/ppermute | solution.py:28
Sparse Core Ops, SparseCore 0:
  9.8 83.0 all-gather.3
  108.6 69.7 all-gather.5
  233.3 66.6 all-gather.7
where the time goes:
time: 382 us; the launch traced here: 381 us
  waiting for transfers between devices  167 us (44%)
  blocking collectives  97.2 us (25%)
  starting transfers between devices  70 us (18%)
  matrix products  16.9 us (4%)
  between operations  13.8 us (4%)
  other arithmetic  12.8 us (3%)
    all_gather x1, waiting for transfers between devices, key_columns(): lax.all_gather(source_rows, 'tp', axis=0, tiled=True)  83.2 us
    ppermute x18, starting transfers between devices, swapped(): return lax.ppermute(block, axis, route)  57.9 us
    all_gather x3, blocking collectives, project_rows(): shard_rows = lax.all_gather(rows_here, 'tp', axis=0, tiled=True)  50.6 us
    all_to_all x2, blocking collectives, sent_and_summed(): lax.all_to_all(parts, axis, split_axis=0, concat_axis=0, tiled=True)  46.6 us
    all_gather x2, waiting for transfers between devices, in_one_piece(): result, at, done = (lax.all_gather(both, axis, axis=dim, tiled=True), 0, [])  42 us
    ppermute x18, waiting for transfers between devices, swapped(): return lax.ppermute(block, axis, route)  26.6 us
    all_to_all x1, waiting for transfers between devices, sent_and_summed(): lax.all_to_all(parts, axis, split_axis=0, concat_axis=0, tiled=True)  13.9 us
  transfers between devices with their start and end apart: 24, of which 16 were waited for; matrix products, arithmetic and copies ran while one was open for 2% of the time, Pallas kernels for 0%

commit v1 on v0

--- a/solution.py
+++ b/solution.py
@@ -2,6 +2,7 @@
 import jax.numpy as jnp
 from jax import lax
 from jax.sharding import PartitionSpec as P
+from jax.lax import axis_index, axis_size, ppermute
 
 HEAD = 128
 KVH = 4
@@ -49,7 +50,30 @@
 
 
 def project_rows(rows_here, weights):
-    shard_rows = lax.all_gather(rows_here, "tp", axis=0, tiled=True)
+    t1 = axis_size("tp")
+    even, then, mat_out = (t1, axis_index("tp"), rows_here.shape[0])
+    history = []
+    for nth in range(even):
+        history.append((nth, (nth + 1) % even))
+    pool = []
+    for nth in range(even):
+        pool.append((nth, (nth - 1) % even))
+    shard_rows = jnp.zeros(
+        (*rows_here.shape[:0], even * mat_out, *rows_here.shape[1:]), rows_here.dtype
+    )
+    shard_rows = lax.dynamic_update_slice_in_dim(shard_rows, rows_here, then * mat_out, axis=0)
+    val2 = y1 = rows_here
+    out_arr = even // 2
+    for t in range(1, out_arr + 1):
+        val2 = ppermute(val2, axis_name="tp", perm=history)
+        shard_rows = lax.dynamic_update_slice_in_dim(
+            shard_rows, val2, (then - t) % even * mat_out, axis=0
+        )
+        if t < even - out_arr:
+            y1 = ppermute(y1, axis_name="tp", perm=pool)
+            shard_rows = lax.dynamic_update_slice_in_dim(
+                shard_rows, y1, (then + t) % even * mat_out, axis=0
+            )
     products = [
         jnp.dot(shard_rows, weight, preferred_element_type=jnp.float32).astype(jnp.bfloat16)
         for weight in weights

time: 382 us -> 441 us (1.15)
  starting transfers between devices: 70 us -> 164 us
  blocking collectives: 97.2 us -> 24.1 us
  waiting for transfers between devices: 167 us -> 207 us
    ppermute x0 -> x45, starting transfers between devices: none -> 65.1 us  [the longest x21 44.9 us: project_rows(): y1 = ppermute(y1, axis_name='tp', perm=pool)]
    all_gather x3 -> x0, blocking collectives: 50.6 us -> none  [project_rows(): shard_rows = lax.all_gather(rows_here, 'tp', axis=0, tiled=True)]
    ppermute x0 -> x45, waiting for transfers between devices: none -> 31.1 us  [the longest x24 25.7 us: project_rows(): val2 = ppermute(val2, axis_name='tp', perm=history)]
    all_to_all x2 -> x1, blocking collectives: 46.6 us -> 24.1 us  [sent_and_summed(): lax.all_to_all(parts, axis, split_axis=0, concat_axis=0, tiled=True)]
    all_to_all x1 -> x2, waiting for transfers between devices: 13.9 us -> 33.6 us  [sent_and_summed(): lax.all_to_all(parts, axis, split_axis=0, concat_axis=0, tiled=True)]
    ppermute x18, starting transfers between devices: 57.9 us -> 77.4 us  [swapped(): return lax.ppermute(block, axis, route)]
    all_to_all x1 -> x2, starting transfers between devices: 6.52 us -> 16.2 us  [sent_and_summed(): lax.all_to_all(parts, axis, split_axis=0, concat_axis=0, tiled=True)]
    all_gather x2, waiting for transfers between devices: 42 us -> 36.3 us  [in_one_piece(): result, at, done = (lax.all_gather(both, axis, axis=dim, tiled=True), 0, [])]
  transfers between devices with their start and end apart: 24 -> 70, of which waited for: 16 -> 59; matrix products, arithmetic and copies ran while one was open for 2% -> 1% of each run, Pallas kernels for 0% -> 0%
where the time goes in v1:
time: 441 us; the launch traced here: 440 us
  waiting for transfers between devices  207 us (47%)
  starting transfers between devices  164 us (37%)
  blocking collectives  24.1 us (5%)
  matrix products  17.9 us (4%)
  between operations  14 us (3%)
  other arithmetic  12.2 us (3%)
    all_gather x1, waiting for transfers between devices, key_columns(): lax.all_gather(source_rows, 'tp', axis=0, tiled=True)  83.2 us
    ppermute x18, starting transfers between devices, swapped(): return lax.ppermute(block, axis, route)  77.4 us
    ppermute x21, starting transfers between devices, project_rows(): y1 = ppermute(y1, axis_name='tp', perm=pool)  44.9 us
    all_gather x2, waiting for transfers between devices, in_one_piece(): result, at, done = (lax.all_gather(both, axis, axis=dim, tiled=True), 0, [])  36.3 us
    all_to_all x2, waiting for transfers between devices, sent_and_summed(): lax.all_to_all(parts, axis, split_axis=0, concat_axis=0, tiled=True)  33.6 us
    ppermute x24, waiting for transfers between devices, project_rows(): val2 = ppermute(val2, axis_name='tp', perm=history)  25.7 us
    all_to_all x1, blocking collectives, sent_and_summed(): lax.all_to_all(parts, axis, split_axis=0, concat_axis=0, tiled=True)  24.1 us
    ppermute x18, waiting for transfers between devices, swapped(): return lax.ppermute(block, axis, route)  21.7 us
  transfers between devices with their start and end apart: 70, of which 59 were waited for; matrix products, arithmetic and copies ran while one was open for 1% of the time, Pallas kernels for 0%

profile of v1, /device:TPU:65, one launch (start us, length us, event | category | flops | bytes accessed | tf_op | source)
XLA Modules:
  0.0 440.4 jit_solution(9529758403261810134)
XLA Ops:
  7.8 1.8 fusion.21
  9.8 83.2 %all-gather.4.cloned.1.call-done = bf16[1024,2048]{1,0:T(8,128)(2,1)} async-done(((bf16[64,2048]{1,0:T(8,128)(2,1)}), bf16[1024,2048]{1,0:T(8,128)(2,1)}) %all-gather.4.cloned.1.call-update) | async-done | bytes 4194320 | tf_op jit(solution)/shard_map/all_gather | solution.py:94
  92.9 3.9 convolution_convert_fusion.3
  96.9 2.2 collective-permute-start.17
  100.2 3.0 collective-permute-start.18
  103.3 3.6 collective-permute-done.18
  107.9 2.1 collective-permute-start
  111.1 2.3 collective-permute-start.2
  114.4 2.3 collective-permute-start.4
  120.1 2.7 collective-permute-start.7
  123.6 3.7 collective-permute-start.9
  128.2 3.7 collective-permute-start.11
  132.7 4.1 collective-permute-start.13
  137.7 4.0 collective-permute-done.14
  142.0 5.8 %collective-permute-start.15 = (bf16[128,128]{0,1:T(8,128)(2,1)S(1)}, bf16[128,128]{0,1:T(8,128)(2,1)S(1)}, u32[]{:S(2)}, u32[]{:S(2)}) collective-permute-start(bf16[128,128]{0,1:T(8,128)(2,1)S(1)} %convolution_convert_fusion.7), channel_id=1, source_target_pairs={{0,1},{1,0},{2,3},{3,2},{4,5},{5,4},{6,7},{7,6},{8,9},{9,8},{10,11... | collective-permute-start | bytes 98312 | tf_op jit(solution)/shard_map/ppermute | solution.py:29
  148.7 2.0 collective-permute-start.16
  150.6 3.1 collective-permute-done.16
  153.7 24.0 %all-gather.6.cloned.1.call-done = bf16[256,4096]{1,0:T(8,128)(2,1)} async-done(((bf16[256,256]{1,0:T(8,128)(2,1)}), bf16[256,4096]{1,0:T(8,128)(2,1)}) %all-gather.6.cloned.1.call-update) | async-done | bytes 2097168 | tf_op jit(solution)/shard_map/all_gather | solution.py:34
  177.7 2.7 multiply_reduce_fusion.1
  180.4 1.5 fusion
  182.0 13.9 %collective-permute-start.19 = (bf16[128,4]{0,1:T(4,128)(2,1)S(1)}, bf16[128,4]{0,1:T(4,128)(2,1)S(1)}, u32[]{:S(2)}, u32[]{:S(2)}) collective-permute-start(bf16[128,4]{0,1:T(4,128)(2,1)S(1)} %get-tuple-element.49), channel_id=1, source_target_pairs={{0,1},{1,0},{2,3},{3,2},{4,5},{5,4},{6,7},{7,6},{8,9},{9,8},{10,11... | collective-permute-start | bytes 3080 | tf_op jit(solution)/shard_map/ppermute | solution.py:29
  196.0 2.0 collective-permute-start.23
  197.9 2.8 collective-permute-start.21
  200.8 2.6 collective-permute-start.24
  203.3 1.8 collective-permute-done.24
  205.1 2.4 fusion.110
  207.6 4.0 collective-permute-start.20
  214.1 2.6 collective-permute-start.22
  216.7 4.0 collective-permute-done.22
  221.9 7.1 %all-to-all-start = ((bf16[16,8,2048]{2,1,0:T(8,128)(2,1)}), bf16[16,8,2048]{2,1,0:T(8,128)(2,1)S(1)}, u32[]{:S(2)}, u32[]{:S(2)}) async-start(bf16[16,8,2048]{2,1,0:T(8,128)(2,1)} %fusion.8), calls=%async_computation | async-start | bytes 1048576 | tf_op jit(solution)/shard_map/all_to_all | solution.py:18
  229.0 17.2 %all-to-all-done = bf16[16,8,2048]{2,1,0:T(8,128)(2,1)S(1)} async-done(((bf16[16,8,2048]{2,1,0:T(8,128)(2,1)}), bf16[16,8,2048]{2,1,0:T(8,128)(2,1)S(1)}, u32[]{:S(2)}, u32[]{:S(2)}) %all-to-all-start) | async-done | bytes 524320 | tf_op jit(solution)/shard_map/all_to_all | solution.py:18
  248.1 2.2 collective-permute-start.27
  251.3 2.3 collective-permute-start.29
  257.3 2.1 collective-permute-start.32
  260.6 3.4 collective-permute-start.34
  264.8 3.7 collective-permute-start.36
  269.4 3.7 collective-permute-start.38
  273.9 4.3 collective-permute-done.39
  278.7 3.3 collective-permute-start.40
  282.5 2.2 collective-permute-start.41
  287.4 9.1 %all-to-all-start.1 = ((bf16[16,8,2048]{2,1,0:T(8,128)(2,1)}), bf16[16,8,2048]{2,1,0:T(8,128)(2,1)S(1)}, u32[]{:S(2)}, u32[]{:S(2)}) async-start(bf16[16,8,2048]{2,1,0:T(8,128)(2,1)} %fusion.9), calls=%async_computation.1 | async-start | bytes 1048576 | tf_op jit(solution)/shard_map/all_to_all | solution.py:18
  297.3 16.4 %all-to-all-done.1 = bf16[16,8,2048]{2,1,0:T(8,128)(2,1)S(1)} async-done(((bf16[16,8,2048]{2,1,0:T(8,128)(2,1)}), bf16[16,8,2048]{2,1,0:T(8,128)(2,1)S(1)}, u32[]{:S(2)}, u32[]{:S(2)}) %all-to-all-start.1) | async-done | bytes 524320 | tf_op jit(solution)/shard_map/all_to_all | solution.py:18
  315.5 2.2 collective-permute-start.44
  318.7 2.3 collective-permute-start.46
  324.7 2.4 collective-permute-start.49
  328.1 3.6 collective-permute-start.51
  332.5 3.7 collective-permute-start.53
  337.1 3.7 collective-permute-start.55
  341.6 4.1 collective-permute-done.56
  346.1 5.8 %collective-permute-start.57 = (bf16[128,128]{0,1:T(8,128)(2,1)S(1)}, bf16[128,128]{0,1:T(8,128)(2,1)S(1)}, u32[]{:S(2)}, u32[]{:S(2)}) collective-permute-start(bf16[128,128]{0,1:T(8,128)(2,1)S(1)} %convolution_convert_fusion.6), channel_id=1, source_target_pairs={{0,1},{1,0},{2,3},{3,2},{4,5},{5,4},{6,7},{7,6},{8,9},{9,8},{10,11... | collective-permute-start | bytes 98312 | tf_op jit(solution)/shard_map/ppermute | solution.py:29
  352.7 2.0 collective-permute-start.58
  354.7 12.4 %all-gather.8.cloned.1.call-done = bf16[256,4096]{1,0:T(8,128)(2,1)} async-done(((bf16[256,256]{1,0:T(8,128)(2,1)}), bf16[256,4096]{1,0:T(8,128)(2,1)}) %all-gather.8.cloned.1.call-update) | async-done | bytes 2097168 | tf_op jit(solution)/shard_map/all_gather | solution.py:34
  367.1 2.7 multiply_reduce_fusion
  369.8 1.5 fusion.2
  371.4 14.8 %collective-permute-start.59 = (bf16[128,4]{0,1:T(4,128)(2,1)S(1)}, bf16[128,4]{0,1:T(4,128)(2,1)S(1)}, u32[]{:S(2)}, u32[]{:S(2)}) collective-permute-start(bf16[128,4]{0,1:T(4,128)(2,1)S(1)} %get-tuple-element.46), channel_id=1, source_target_pairs={{0,1},{1,0},{2,3},{3,2},{4,5},{5,4},{6,7},{7,6},{8,9},{9,8},{10,11... | collective-permute-start | bytes 3080 | tf_op jit(solution)/shard_map/ppermute | solution.py:29
  386.2 2.0 collective-permute-start.63
  388.2 2.5 collective-permute-start.61
  390.7 2.9 collective-permute-start.64
  393.6 1.5 collective-permute-done.64
  395.1 1.7 fusion.111
  396.8 3.9 collective-permute-start.60
  401.8 2.9 collective-permute-start.62
  404.7 3.7 collective-permute-done.62
  408.8 24.1 %all_to_all.15 = bf16[16,8,2048]{2,1,0:T(8,128)(2,1)S(1)} all-to-all(bf16[16,8,2048]{2,1,0:T(8,128)(2,1)S(1)} %fusion.10), channel_id=1, replica_groups=mesh['grp'=2,'sp'=16,'tp'=16] {'tp'}, dimensions={0} | all-to-all | bytes 1048576 | tf_op jit(solution)/shard_map/all_to_all | solution.py:18
  (232 shorter events, 45.6 us)
Async XLA Ops:
  6.6 86.4 %all-gather.4.cloned.1.call-start = ((), (), s32[]{:S(2)}) async-start(), calls=%async_computation.3 | async-start | bytes 4456448 | tf_op jit(solution)/shard_map/all_gather | solution.py:94
  9.7 168.0 %all-gather.6.cloned.1.call-start = ((), (), s32[]{:S(2)}) async-start(), calls=%async_computation.4 | async-start | bytes 2228224 | tf_op jit(solution)/shard_map/all_gather | solution.py:34
  100.2 6.7 %collective-permute-start.18 = (bf16[2,128,256]{2,1,0:T(8,128)(2,1)S(1)}, bf16[2,128,256]{2,1,0:T(8,128)(2,1)S(1)}, u32[]{:S(2)}, u32[]{:S(2)}) collective-permute-start(bf16[2,128,256]{2,1,0:T(8,128)(2,1)S(1)} %get-tuple-element.36), channel_id=1, source_target_pairs={{0,2},{2,0},{1,3},{3,1},{4,6},{6,4},{5,7},{7,5},{8,10},{10,8},{9,1... | collective-permute-start | bytes 393224 | tf_op jit(solution)/shard_map/ppermute | solution.py:29
  110.1 3.3 collective-permute-start.1
  111.1 3.3 collective-permute-start.2
  113.4 3.3 collective-permute-start.3
  114.4 4.5 %collective-permute-start.4 = (bf16[8,2048]{1,0:T(8,128)(2,1)S(1)}, bf16[8,2048]{1,0:T(8,128)(2,1)S(1)}, u32[]{:S(2)}, u32[]{:S(2)}) collective-permute-start(bf16[8,2048]{1,0:T(8,128)(2,1)S(1)} %collective-permute-done.2), channel_id=1, source_target_pairs={{0,1},{1,2},{2,3},{3,4},{4,5},{5,6},{6,7},{7,8},{8,9},{9,10},{10,1... | collective-permute-start | bytes 98312 | tf_op jit(solution)/shard_map/ppermute | solution.py:68
  116.7 3.3 collective-permute-start.5
  118.9 4.6 %collective-permute-start.6 = (bf16[8,2048]{1,0:T(8,128)(2,1)S(1)}, bf16[8,2048]{1,0:T(8,128)(2,1)S(1)}, u32[]{:S(2)}, u32[]{:S(2)}) collective-permute-start(bf16[8,2048]{1,0:T(8,128)(2,1)S(1)} %collective-permute-done.4), channel_id=1, source_target_pairs={{0,1},{1,2},{2,3},{3,4},{4,5},{5,6},{6,7},{7,8},{8,9},{9,10},{10,1... | collective-permute-start | bytes 98312 | tf_op jit(solution)/shard_map/ppermute | solution.py:68
  120.1 3.5 collective-permute-start.7
  123.4 4.6 %collective-permute-start.8 = (bf16[8,2048]{1,0:T(8,128)(2,1)S(1)}, bf16[8,2048]{1,0:T(8,128)(2,1)S(1)}, u32[]{:S(2)}, u32[]{:S(2)}) collective-permute-start(bf16[8,2048]{1,0:T(8,128)(2,1)S(1)} %collective-permute-done.6), channel_id=1, source_target_pairs={{0,1},{1,2},{2,3},{3,4},{4,5},{5,6},{6,7},{7,8},{8,9},{9,10},{10,1... | collective-permute-start | bytes 98312 | tf_op jit(solution)/shard_map/ppermute | solution.py:68
  123.6 4.6 %collective-permute-start.9 = (bf16[8,2048]{1,0:T(8,128)(2,1)S(1)}, bf16[8,2048]{1,0:T(8,128)(2,1)S(1)}, u32[]{:S(2)}, u32[]{:S(2)}) collective-permute-start(bf16[8,2048]{1,0:T(8,128)(2,1)S(1)} %collective-permute-done.7), channel_id=1, source_target_pairs={{0,15},{1,0},{2,1},{3,2},{4,3},{5,4},{6,5},{7,6},{8,7},{9,8},{10,9... | collective-permute-start | bytes 98312 | tf_op jit(solution)/shard_map/ppermute | solution.py:73
  128.0 4.6 %collective-permute-start.10 = (bf16[8,2048]{1,0:T(8,128)(2,1)S(1)}, bf16[8,2048]{1,0:T(8,128)(2,1)S(1)}, u32[]{:S(2)}, u32[]{:S(2)}) collective-permute-start(bf16[8,2048]{1,0:T(8,128)(2,1)S(1)} %collective-permute-done.8), channel_id=1, source_target_pairs={{0,1},{1,2},{2,3},{3,4},{4,5},{5,6},{6,7},{7,8},{8,9},{9,10},{10,1... | collective-permute-start | bytes 98312 | tf_op jit(solution)/shard_map/ppermute | solution.py:68
  128.2 4.6 %collective-permute-start.11 = (bf16[8,2048]{1,0:T(8,128)(2,1)S(1)}, bf16[8,2048]{1,0:T(8,128)(2,1)S(1)}, u32[]{:S(2)}, u32[]{:S(2)}) collective-permute-start(bf16[8,2048]{1,0:T(8,128)(2,1)S(1)} %collective-permute-done.9), channel_id=1, source_target_pairs={{0,15},{1,0},{2,1},{3,2},{4,3},{5,4},{6,5},{7,6},{8,7},{9,8},{10,9... | collective-permute-start | bytes 98312 | tf_op jit(solution)/shard_map/ppermute | solution.py:73
  132.5 4.6 %collective-permute-start.12 = (bf16[8,2048]{1,0:T(8,128)(2,1)S(1)}, bf16[8,2048]{1,0:T(8,128)(2,1)S(1)}, u32[]{:S(2)}, u32[]{:S(2)}) collective-permute-start(bf16[8,2048]{1,0:T(8,128)(2,1)S(1)} %collective-permute-done.10), channel_id=1, source_target_pairs={{0,1},{1,2},{2,3},{3,4},{4,5},{5,6},{6,7},{7,8},{8,9},{9,10},{10,1... | collective-permute-start | bytes 98312 | tf_op jit(solution)/shard_map/ppermute | solution.py:68
  132.7 5.0 %collective-permute-start.13 = (bf16[8,2048]{1,0:T(8,128)(2,1)S(1)}, bf16[8,2048]{1,0:T(8,128)(2,1)S(1)}, u32[]{:S(2)}, u32[]{:S(2)}) collective-permute-start(bf16[8,2048]{1,0:T(8,128)(2,1)S(1)} %collective-permute-done.11), channel_id=1, source_target_pairs={{0,15},{1,0},{2,1},{3,2},{4,3},{5,4},{6,5},{7,6},{8,7},{9,8},{10,9... | collective-permute-start | bytes 98312 | tf_op jit(solution)/shard_map/ppermute | solution.py:73
  137.1 4.5 %collective-permute-start.14 = (bf16[8,2048]{1,0:T(8,128)(2,1)S(1)}, bf16[8,2048]{1,0:T(8,128)(2,1)S(1)}, u32[]{:S(2)}, u32[]{:S(2)}) collective-permute-start(bf16[8,2048]{1,0:T(8,128)(2,1)S(1)} %collective-permute-done.12), channel_id=1, source_target_pairs={{0,1},{1,2},{2,3},{3,4},{4,5},{5,6},{6,7},{7,8},{8,9},{9,10},{10,1... | collective-permute-start | bytes 98312 | tf_op jit(solution)/shard_map/ppermute | solution.py:68
  142.0 6.6 %collective-permute-start.15 = (bf16[128,128]{0,1:T(8,128)(2,1)S(1)}, bf16[128,128]{0,1:T(8,128)(2,1)S(1)}, u32[]{:S(2)}, u32[]{:S(2)}) collective-permute-start(bf16[128,128]{0,1:T(8,128)(2,1)S(1)} %convolution_convert_fusion.7), channel_id=1, source_target_pairs={{0,1},{1,0},{2,3},{3,2},{4,5},{5,4},{6,7},{7,6},{8,9},{9,8},{10,11... | collective-permute-start | bytes 98312 | tf_op jit(solution)/shard_map/ppermute | solution.py:29
  148.7 5.0 %collective-permute-start.16 = (bf16[128,256]{0,1:T(8,128)(2,1)S(1)}, bf16[128,256]{0,1:T(8,128)(2,1)S(1)}, u32[]{:S(2)}, u32[]{:S(2)}) collective-permute-start(bf16[128,256]{0,1:T(8,128)(2,1)S(1)} %maximum_select_fusion.7), channel_id=1, source_target_pairs={{0,2},{2,0},{1,3},{3,1},{4,6},{6,4},{5,7},{7,5},{8,10},{10,8},{9,1... | collective-permute-start | bytes 196616 | tf_op jit(solution)/shard_map/ppermute | solution.py:29
  182.0 15.9 %collective-permute-start.19 = (bf16[128,4]{0,1:T(4,128)(2,1)S(1)}, bf16[128,4]{0,1:T(4,128)(2,1)S(1)}, u32[]{:S(2)}, u32[]{:S(2)}) collective-permute-start(bf16[128,4]{0,1:T(4,128)(2,1)S(1)} %get-tuple-element.49), channel_id=1, source_target_pairs={{0,1},{1,0},{2,3},{3,2},{4,5},{5,4},{6,7},{7,6},{8,9},{9,8},{10,11... | collective-permute-start | bytes 3080 | tf_op jit(solution)/shard_map/ppermute | solution.py:29
  196.0 4.8 %collective-permute-start.23 = (bf16[128,4]{0,1:T(4,128)(2,1)S(1)}, bf16[128,4]{0,1:T(4,128)(2,1)S(1)}, u32[]{:S(2)}, u32[]{:S(2)}) collective-permute-start(bf16[128,4]{0,1:T(4,128)(2,1)S(1)} %get-tuple-element.50), channel_id=1, source_target_pairs={{0,1},{1,0},{2,3},{3,2},{4,5},{5,4},{6,7},{7,6},{8,9},{9,8},{10,11... | collective-permute-start | bytes 3080 | tf_op jit(solution)/shard_map/ppermute | solution.py:29
  197.9 5.4 %collective-permute-start.21 = (bf16[128,4]{0,1:T(4,128)(2,1)S(1)}, bf16[128,4]{0,1:T(4,128)(2,1)S(1)}, u32[]{:S(2)}, u32[]{:S(2)}) collective-permute-start(bf16[128,4]{0,1:T(4,128)(2,1)S(1)} %fusion.82), channel_id=1, source_target_pairs={{0,2},{2,0},{1,3},{3,1},{4,6},{6,4},{5,7},{7,5},{8,10},{10,8},{9,1... | collective-permute-start | bytes 3080 | tf_op jit(solution)/shard_map/ppermute | solution.py:29
  200.8 4.3 collective-permute-start.24
  207.6 5.3 %collective-permute-start.20 = (bf16[128,4,128]{2,0,1:T(8,128)(2,1)}, bf16[128,4,128]{2,0,1:T(8,128)(2,1)}, u32[]{:S(2)}, u32[]{:S(2)}) collective-permute-start(bf16[128,4,128]{2,0,1:T(8,128)(2,1)} %get-tuple-element.53), channel_id=1, source_target_pairs={{0,1},{1,0},{2,3},{3,2},{4,5},{5,4},{6,7},{7,6},{8,9},{9,8},{10,11... | collective-permute-start | bytes 393224 | tf_op jit(solution)/shard_map/ppermute | solution.py:29
  214.1 6.6 %collective-permute-start.22 = (bf16[128,4,128]{2,0,1:T(8,128)(2,1)S(1)}, bf16[128,4,128]{2,0,1:T(8,128)(2,1)S(1)}, u32[]{:S(2)}, u32[]{:S(2)}) collective-permute-start(bf16[128,4,128]{2,0,1:T(8,128)(2,1)S(1)} %get-tuple-element.27), channel_id=1, source_target_pairs={{0,2},{2,0},{1,3},{3,1},{4,6},{6,4},{5,7},{7,5},{8,10},{10,8},{9,1... | collective-permute-start | bytes 393224 | tf_op jit(solution)/shard_map/ppermute | solution.py:29
  221.9 24.3 %all-to-all-start = ((bf16[16,8,2048]{2,1,0:T(8,128)(2,1)}), bf16[16,8,2048]{2,1,0:T(8,128)(2,1)S(1)}, u32[]{:S(2)}, u32[]{:S(2)}) async-start(bf16[16,8,2048]{2,1,0:T(8,128)(2,1)} %fusion.8), calls=%async_computation | async-start | bytes 1048576 | tf_op jit(solution)/shard_map/all_to_all | solution.py:18
  246.9 3.4 collective-permute-start.26
  250.3 3.6 collective-permute-start.28
  251.3 4.3 collective-permute-start.29
  253.9 3.3 collective-permute-start.30
  255.5 4.6 %collective-permute-start.31 = (bf16[8,2048]{1,0:T(8,128)(2,1)S(1)}, bf16[8,2048]{1,0:T(8,128)(2,1)S(1)}, u32[]{:S(2)}, u32[]{:S(2)}) collective-permute-start(bf16[8,2048]{1,0:T(8,128)(2,1)S(1)} %collective-permute-done.29), channel_id=1, source_target_pairs={{0,1},{1,2},{2,3},{3,4},{4,5},{5,6},{6,7},{7,8},{8,9},{9,10},{10,1... | collective-permute-start | bytes 98312 | tf_op jit(solution)/shard_map/ppermute | solution.py:68
  257.3 3.3 collective-permute-start.32
  260.1 4.6 %collective-permute-start.33 = (bf16[8,2048]{1,0:T(8,128)(2,1)S(1)}, bf16[8,2048]{1,0:T(8,128)(2,1)S(1)}, u32[]{:S(2)}, u32[]{:S(2)}) collective-permute-start(bf16[8,2048]{1,0:T(8,128)(2,1)S(1)} %collective-permute-done.31), channel_id=1, source_target_pairs={{0,1},{1,2},{2,3},{3,4},{4,5},{5,6},{6,7},{7,8},{8,9},{9,10},{10,1... | collective-permute-start | bytes 98312 | tf_op jit(solution)/shard_map/ppermute | solution.py:68
  260.6 4.2 collective-permute-start.34
  264.6 4.6 %collective-permute-start.35 = (bf16[8,2048]{1,0:T(8,128)(2,1)S(1)}, bf16[8,2048]{1,0:T(8,128)(2,1)S(1)}, u32[]{:S(2)}, u32[]{:S(2)}) collective-permute-start(bf16[8,2048]{1,0:T(8,128)(2,1)S(1)} %collective-permute-done.33), channel_id=1, source_target_pairs={{0,1},{1,2},{2,3},{3,4},{4,5},{5,6},{6,7},{7,8},{8,9},{9,10},{10,1... | collective-permute-start | bytes 98312 | tf_op jit(solution)/shard_map/ppermute | solution.py:68
  264.8 4.6 %collective-permute-start.36 = (bf16[8,2048]{1,0:T(8,128)(2,1)S(1)}, bf16[8,2048]{1,0:T(8,128)(2,1)S(1)}, u32[]{:S(2)}, u32[]{:S(2)}) collective-permute-start(bf16[8,2048]{1,0:T(8,128)(2,1)S(1)} %collective-permute-done.34), channel_id=1, source_target_pairs={{0,15},{1,0},{2,1},{3,2},{4,3},{5,4},{6,5},{7,6},{8,7},{9,8},{10,9... | collective-permute-start | bytes 98312 | tf_op jit(solution)/shard_map/ppermute | solution.py:73
  269.2 4.6 %collective-permute-start.37 = (bf16[8,2048]{1,0:T(8,128)(2,1)S(1)}, bf16[8,2048]{1,0:T(8,128)(2,1)S(1)}, u32[]{:S(2)}, u32[]{:S(2)}) collective-permute-start(bf16[8,2048]{1,0:T(8,128)(2,1)S(1)} %collective-permute-done.35), channel_id=1, source_target_pairs={{0,1},{1,2},{2,3},{3,4},{4,5},{5,6},{6,7},{7,8},{8,9},{9,10},{10,1... | collective-permute-start | bytes 98312 | tf_op jit(solution)/shard_map/ppermute | solution.py:68
  269.4 4.6 %collective-permute-start.38 = (bf16[8,2048]{1,0:T(8,128)(2,1)S(1)}, bf16[8,2048]{1,0:T(8,128)(2,1)S(1)}, u32[]{:S(2)}, u32[]{:S(2)}) collective-permute-start(bf16[8,2048]{1,0:T(8,128)(2,1)S(1)} %collective-permute-done.36), channel_id=1, source_target_pairs={{0,15},{1,0},{2,1},{3,2},{4,3},{5,4},{6,5},{7,6},{8,7},{9,8},{10,9... | collective-permute-start | bytes 98312 | tf_op jit(solution)/shard_map/ppermute | solution.py:73
  273.7 4.6 %collective-permute-start.39 = (bf16[8,2048]{1,0:T(8,128)(2,1)S(1)}, bf16[8,2048]{1,0:T(8,128)(2,1)S(1)}, u32[]{:S(2)}, u32[]{:S(2)}) collective-permute-start(bf16[8,2048]{1,0:T(8,128)(2,1)S(1)} %collective-permute-done.37), channel_id=1, source_target_pairs={{0,1},{1,2},{2,3},{3,4},{4,5},{5,6},{6,7},{7,8},{8,9},{9,10},{10,1... | collective-permute-start | bytes 98312 | tf_op jit(solution)/shard_map/ppermute | solution.py:68
  278.7 6.0 %collective-permute-start.40 = (bf16[2,176]{0,1:T(8,128)(2,1)S(1)}, bf16[2,176]{0,1:T(8,128)(2,1)S(1)}, u32[]{:S(2)}, u32[]{:S(2)}) collective-permute-start(bf16[2,176]{0,1:T(8,128)(2,1)S(1)} %slice.122), channel_id=1, source_target_pairs={{0,16},{16,32},{32,48},{48,64},{64,80},{80,96},{96,112},{112,128},... | collective-permute-start | bytes 2120 | tf_op jit(solution)/shard_map/ppermute | solution.py:44
  282.5 3.3 collective-permute-start.41
  287.4 26.4 %all-to-all-start.1 = ((bf16[16,8,2048]{2,1,0:T(8,128)(2,1)}), bf16[16,8,2048]{2,1,0:T(8,128)(2,1)S(1)}, u32[]{:S(2)}, u32[]{:S(2)}) async-start(bf16[16,8,2048]{2,1,0:T(8,128)(2,1)} %fusion.9), calls=%async_computation.1 | async-start | bytes 1048576 | tf_op jit(solution)/shard_map/all_to_all | solution.py:18
  296.5 70.6 %all-gather.8.cloned.1.call-start = ((), (), s32[]{:S(2)}) async-start(), calls=%async_computation.5 | async-start | bytes 2228224 | tf_op jit(solution)/shard_map/all_gather | solution.py:34
  314.4 3.4 collective-permute-start.43
  317.7 3.6 collective-permute-start.45
  318.7 4.3 collective-permute-start.46
  321.4 3.3 collective-permute-start.47
  323.0 4.5 %collective-permute-start.48 = (bf16[8,2048]{1,0:T(8,128)(2,1)S(1)}, bf16[8,2048]{1,0:T(8,128)(2,1)S(1)}, u32[]{:S(2)}, u32[]{:S(2)}) collective-permute-start(bf16[8,2048]{1,0:T(8,128)(2,1)S(1)} %collective-permute-done.46), channel_id=1, source_target_pairs={{0,1},{1,2},{2,3},{3,4},{4,5},{5,6},{6,7},{7,8},{8,9},{9,10},{10,1... | collective-permute-start | bytes 98312 | tf_op jit(solution)/shard_map/ppermute | solution.py:68
  324.7 3.3 collective-permute-start.49
  327.5 4.6 %collective-permute-start.50 = (bf16[8,2048]{1,0:T(8,128)(2,1)S(1)}, bf16[8,2048]{1,0:T(8,128)(2,1)S(1)}, u32[]{:S(2)}, u32[]{:S(2)}) collective-permute-start(bf16[8,2048]{1,0:T(8,128)(2,1)S(1)} %collective-permute-done.48), channel_id=1, source_target_pairs={{0,1},{1,2},{2,3},{3,4},{4,5},{5,6},{6,7},{7,8},{8,9},{9,10},{10,1... | collective-permute-start | bytes 98312 | tf_op jit(solution)/shard_map/ppermute | solution.py:68
  328.1 4.5 %collective-permute-start.51 = (bf16[8,2048]{1,0:T(8,128)(2,1)S(1)}, bf16[8,2048]{1,0:T(8,128)(2,1)S(1)}, u32[]{:S(2)}, u32[]{:S(2)}) collective-permute-start(bf16[8,2048]{1,0:T(8,128)(2,1)S(1)} %collective-permute-done.49), channel_id=1, source_target_pairs={{0,15},{1,0},{2,1},{3,2},{4,3},{5,4},{6,5},{7,6},{8,7},{9,8},{10,9... | collective-permute-start | bytes 98312 | tf_op jit(solution)/shard_map/ppermute | solution.py:73
  332.1 4.6 %collective-permute-start.52 = (bf16[8,2048]{1,0:T(8,128)(2,1)S(1)}, bf16[8,2048]{1,0:T(8,128)(2,1)S(1)}, u32[]{:S(2)}, u32[]{:S(2)}) collective-permute-start(bf16[8,2048]{1,0:T(8,128)(2,1)S(1)} %collective-permute-done.50), channel_id=1, source_target_pairs={{0,1},{1,2},{2,3},{3,4},{4,5},{5,6},{6,7},{7,8},{8,9},{9,10},{10,1... | collective-permute-start | bytes 98312 | tf_op jit(solution)/shard_map/ppermute | solution.py:68
  332.5 4.6 %collective-permute-start.53 = (bf16[8,2048]{1,0:T(8,128)(2,1)S(1)}, bf16[8,2048]{1,0:T(8,128)(2,1)S(1)}, u32[]{:S(2)}, u32[]{:S(2)}) collective-permute-start(bf16[8,2048]{1,0:T(8,128)(2,1)S(1)} %collective-permute-done.51), channel_id=1, source_target_pairs={{0,15},{1,0},{2,1},{3,2},{4,3},{5,4},{6,5},{7,6},{8,7},{9,8},{10,9... | collective-permute-start | bytes 98312 | tf_op jit(solution)/shard_map/ppermute | solution.py:73
  336.6 4.6 %collective-permute-start.54 = (bf16[8,2048]{1,0:T(8,128)(2,1)S(1)}, bf16[8,2048]{1,0:T(8,128)(2,1)S(1)}, u32[]{:S(2)}, u32[]{:S(2)}) collective-permute-start(bf16[8,2048]{1,0:T(8,128)(2,1)S(1)} %collective-permute-done.52), channel_id=1, source_target_pairs={{0,1},{1,2},{2,3},{3,4},{4,5},{5,6},{6,7},{7,8},{8,9},{9,10},{10,1... | collective-permute-start | bytes 98312 | tf_op jit(solution)/shard_map/ppermute | solution.py:68
  337.1 4.6 %collective-permute-start.55 = (bf16[8,2048]{1,0:T(8,128)(2,1)S(1)}, bf16[8,2048]{1,0:T(8,128)(2,1)S(1)}, u32[]{:S(2)}, u32[]{:S(2)}) collective-permute-start(bf16[8,2048]{1,0:T(8,128)(2,1)S(1)} %collective-permute-done.53), channel_id=1, source_target_pairs={{0,15},{1,0},{2,1},{3,2},{4,3},{5,4},{6,5},{7,6},{8,7},{9,8},{10,9... | collective-permute-start | bytes 98312 | tf_op jit(solution)/shard_map/ppermute | solution.py:73
  341.2 4.6 %collective-permute-start.56 = (bf16[8,2048]{1,0:T(8,128)(2,1)S(1)}, bf16[8,2048]{1,0:T(8,128)(2,1)S(1)}, u32[]{:S(2)}, u32[]{:S(2)}) collective-permute-start(bf16[8,2048]{1,0:T(8,128)(2,1)S(1)} %collective-permute-done.54), channel_id=1, source_target_pairs={{0,1},{1,2},{2,3},{3,4},{4,5},{5,6},{6,7},{7,8},{8,9},{9,10},{10,1... | collective-permute-start | bytes 98312 | tf_op jit(solution)/shard_map/ppermute | solution.py:68
  346.1 6.6 %collective-permute-start.57 = (bf16[128,128]{0,1:T(8,128)(2,1)S(1)}, bf16[128,128]{0,1:T(8,128)(2,1)S(1)}, u32[]{:S(2)}, u32[]{:S(2)}) collective-permute-start(bf16[128,128]{0,1:T(8,128)(2,1)S(1)} %convolution_convert_fusion.6), channel_id=1, source_target_pairs={{0,1},{1,0},{2,3},{3,2},{4,5},{5,4},{6,7},{7,6},{8,9},{9,8},{10,11... | collective-permute-start | bytes 98312 | tf_op jit(solution)/shard_map/ppermute | solution.py:29
  352.7 14.3 %collective-permute-start.58 = (bf16[128,256]{0,1:T(8,128)(2,1)S(1)}, bf16[128,256]{0,1:T(8,128)(2,1)S(1)}, u32[]{:S(2)}, u32[]{:S(2)}) collective-permute-start(bf16[128,256]{0,1:T(8,128)(2,1)S(1)} %maximum_select_fusion.9), channel_id=1, source_target_pairs={{0,2},{2,0},{1,3},{3,1},{4,6},{6,4},{5,7},{7,5},{8,10},{10,8},{9,1... | collective-permute-start | bytes 196616 | tf_op jit(solution)/shard_map/ppermute | solution.py:29
  371.4 16.8 %collective-permute-start.59 = (bf16[128,4]{0,1:T(4,128)(2,1)S(1)}, bf16[128,4]{0,1:T(4,128)(2,1)S(1)}, u32[]{:S(2)}, u32[]{:S(2)}) collective-permute-start(bf16[128,4]{0,1:T(4,128)(2,1)S(1)} %get-tuple-element.46), channel_id=1, source_target_pairs={{0,1},{1,0},{2,3},{3,2},{4,5},{5,4},{6,7},{7,6},{8,9},{9,8},{10,11... | collective-permute-start | bytes 3080 | tf_op jit(solution)/shard_map/ppermute | solution.py:29
  386.2 4.5 %collective-permute-start.63 = (bf16[128,4]{0,1:T(4,128)(2,1)S(1)}, bf16[128,4]{0,1:T(4,128)(2,1)S(1)}, u32[]{:S(2)}, u32[]{:S(2)}) collective-permute-start(bf16[128,4]{0,1:T(4,128)(2,1)S(1)} %get-tuple-element.47), channel_id=1, source_target_pairs={{0,1},{1,0},{2,3},{3,2},{4,5},{5,4},{6,7},{7,6},{8,9},{9,8},{10,11... | collective-permute-start | bytes 3080 | tf_op jit(solution)/shard_map/ppermute | solution.py:29
  388.2 5.4 %collective-permute-start.61 = (bf16[128,4]{0,1:T(4,128)(2,1)S(1)}, bf16[128,4]{0,1:T(4,128)(2,1)S(1)}, u32[]{:S(2)}, u32[]{:S(2)}) collective-permute-start(bf16[128,4]{0,1:T(4,128)(2,1)S(1)} %fusion.83), channel_id=1, source_target_pairs={{0,2},{2,0},{1,3},{3,1},{4,6},{6,4},{5,7},{7,5},{8,10},{10,8},{9,1... | collective-permute-start | bytes 3080 | tf_op jit(solution)/shard_map/ppermute | solution.py:29
  390.7 4.3 collective-permute-start.64
  396.8 4.8 %collective-permute-start.60 = (bf16[128,4,128]{2,0,1:T(8,128)(2,1)S(1)}, bf16[128,4,128]{2,0,1:T(8,128)(2,1)S(1)}, u32[]{:S(2)}, u32[]{:S(2)}) collective-permute-start(bf16[128,4,128]{2,0,1:T(8,128)(2,1)S(1)} %get-tuple-element.57), channel_id=1, source_target_pairs={{0,1},{1,0},{2,3},{3,2},{4,5},{5,4},{6,7},{7,6},{8,9},{9,8},{10,11... | collective-permute-start | bytes 393224 | tf_op jit(solution)/shard_map/ppermute | solution.py:29
  401.8 6.6 %collective-permute-start.62 = (bf16[128,4,128]{2,0,1:T(8,128)(2,1)S(1)}, bf16[128,4,128]{2,0,1:T(8,128)(2,1)S(1)}, u32[]{:S(2)}, u32[]{:S(2)}) collective-permute-start(bf16[128,4,128]{2,0,1:T(8,128)(2,1)S(1)} %get-tuple-element.12), channel_id=1, source_target_pairs={{0,2},{2,0},{1,3},{3,1},{4,6},{6,4},{5,7},{7,5},{8,10},{10,8},{9,1... | collective-permute-start | bytes 393224 | tf_op jit(solution)/shard_map/ppermute | solution.py:29
  (24 other events, 1594.1 us)
Sparse Core Ops, SparseCore 0:
  9.8 83.0 all-gather.3
  107.9 69.7 all-gather.5
  299.4 67.6 all-gather.7
